TPU v7x, 32 devices: a whole 2x2x4 slice. The times are simulated.
32 devices in a mesh: sp: 16 (over z, y, x), tp: 2 (over core).
Axes of the slice: x: 2, y: 2, z: 4, core: 2. Of those that a mesh axis runs over, the one named last changes fastest.
Arguments:
- inputs: bfloat16 [4096, 2048], P('sp', 'tp'), may hold values from -200 to 200
- input_gain: bfloat16 [2048], P('tp'), may hold values from 0.099609375 to 1.8984375
- stick_query_w: bfloat16 [2048, 1024], P(None, 'tp'), may hold values from -0.3125 to 0.3125
- stick_key_w: bfloat16 [2048, 1024], P(None, 'tp'), may hold values from -0.125 to 0.125
- stick_value_w: bfloat16 [2048, 1024], P(None, 'tp'), may hold values from -0.125 to 0.125
- ret_query_w: bfloat16 [2048, 2048], P(None, 'tp'), may hold values from -0.125 to 0.125
- ret_key_w: bfloat16 [2048, 2048], P(None, 'tp'), may hold values from -0.125 to 0.125
- ret_value_w: bfloat16 [2048, 2048], P(None, 'tp'), may hold values from -0.125 to 0.125
- stick_offset: float32 [8], P('tp'), may hold values from -17 to -2
- ret_log_decay: float32 [8], P('tp'), may hold values from -0.04 to 0, as said below
- initial_state: float32 [8, 256, 256], P('tp', 'sp'), may hold values from -38.4 to 38.4
- stick_gain: float32 [1024], P('tp'), may hold values from 0.1 to 1.9
- ret_gain: float32 [2048], P('tp'), may hold values from 0.1 to 1.9
- stick_out_w: bfloat16 [1024, 2048], P('tp', 'sp'), may hold values from -0.125 to 0.125
- ret_out_w: bfloat16 [2048, 2048], P('tp', 'sp'), may hold values from -0.09375 to 0.09375
Outputs:
- layer_out: bfloat16 [4096, 2048], P(('sp', 'tp'))
Inputs may be any that keep to these rules, and one draw needn't show every extreme that they name: `ret_log_decay`: every entry is negative.
All inputs are finite; a program needn't handle non-finite values.
Results may differ from a plain program's by a relative error of at most 0.017.
Values may be sent and summed in bfloat16 or wider, within the bound.
A program may use at most 128 MiB of HBM per device.

v0:
```python
import jax
import jax.numpy as jnp
from jax import lax
from jax.sharding import PartitionSpec as P

D = 2048
STICK_HEADS = 8
STICK_DIM = 128
epsilon = 1e-06
rope_base = 10000.0


def entering_2(value, axis, join, neutral):
    count, mine = (lax.axis_size(axis), lax.axis_index(axis))
    pieces = jax.tree.map(lambda part: lax.all_gather(part, axis), value)
    running = jax.tree.map(
        lambda part, zero: jnp.full_like(part, 0) + jnp.asarray(zero, part.dtype), value, neutral
    )

    def hop(position, running):
        longer = join(running, jax.tree.map(lambda part: part[position], pieces))
        return jax.tree.map(lambda new, old: jnp.where(position < mine, new, old), longer, running)

    return lax.fori_loop(0, count - 1, hop, running)


def rotate(values, positions):
    half_width = values.shape[-1] // 2
    inverse = rope_base ** (-jnp.arange(half_width, dtype=jnp.float32) / half_width)
    angles = positions.astype(jnp.float32)[:, None] * inverse[None, :]
    cosine = jnp.cos(angles)[:, None, :]
    sine_table = jnp.sin(angles)[:, None, :]
    first_half = values[..., :half_width]
    second_half = values[..., half_width:]
    return jnp.concatenate(
        [
            first_half * cosine - second_half * sine_table,
            second_half * cosine + first_half * sine_table,
        ],
        axis=-1,
    )


def stick_block(partial_state, queries, key_rows, value_rows, offsets, query_pos, key_pos):
    running, before = partial_state
    score_scale = queries.shape[2] ** (-0.5)
    scores = (
        jnp.einsum("thd,shd->hts", queries, key_rows, preferred_element_type=jnp.float32)
        * score_scale
        + offsets[:, None, None]
    )
    allowed = ((key_pos[None, :] < query_pos[:, None]) & (key_pos[None, :] >= 0))[None]
    remain = jnp.where(allowed, jax.nn.log_sigmoid(-scores), 0.0)
    suffix = lax.cumsum(remain, axis=2, reverse=True) - remain + before[:, :, None]
    weights = jnp.where(allowed, jnp.exp(jax.nn.log_sigmoid(scores) + suffix), 0.0).astype(
        jnp.bfloat16
    )
    running = running + jnp.einsum(
        "hts,shd->thd", weights, value_rows, preferred_element_type=jnp.float32
    )
    return (running, before + jnp.sum(remain, axis=2))


def sweep_keys(keys_all, values_all, query_rows, positions, offsets, key_span):
    row_count, head_count, head_width = query_rows.shape
    span_offsets = jnp.arange(key_span, dtype=jnp.int32)
    needed = (positions[row_count - 1] + key_span) // key_span

    def visit(visit_index, partial_state):
        key_start = (needed - 1 - visit_index) * key_span
        key_rows = lax.dynamic_slice_in_dim(keys_all, key_start, key_span, 0).reshape(
            key_span, head_count, head_width
        )
        value_rows = lax.dynamic_slice_in_dim(values_all, key_start, key_span, 0).reshape(
            key_span, head_count, head_width
        )
        return stick_block(
            partial_state,
            query_rows,
            key_rows,
            value_rows,
            offsets,
            positions,
            key_start + span_offsets,
        )

    start_carry = (
        jnp.zeros((row_count, head_count, head_width), jnp.float32),
        jnp.zeros((head_count, row_count), jnp.float32),
    )
    final_state = lax.fori_loop(0, needed, visit, start_carry)
    return final_state[0]


def body(
    inputs,
    input_gain,
    stick_query_w,
    stick_key_w,
    stick_value_w,
    ret_query_w,
    ret_key_w,
    ret_value_w,
    stick_offset,
    ret_log_decay,
    initial_state,
    stick_gain,
    ret_gain,
    stick_out_w,
    ret_out_w,
):
    tok_rows = inputs.shape[0]
    matrices = (stick_query_w, stick_key_w, stick_value_w, ret_query_w, ret_key_w, ret_value_w)
    own_squares = jnp.sum(jnp.square(inputs.astype(jnp.float32)), axis=1)
    squares = lax.psum(own_squares, "tp")
    scaled = (
        lax.all_gather(inputs, "tp", axis=1, tiled=True).astype(jnp.float32)
        * lax.all_gather(input_gain[None, :], "tp", axis=1, tiled=True).astype(jnp.float32)
    ).astype(jnp.bfloat16)
    projected = tuple(
        (jnp.dot(scaled, matrix, preferred_element_type=jnp.float32) for matrix in matrices)
    )
    row_scale = lax.rsqrt(squares / D + epsilon)
    stick_query, stick_key, stick_value, ret_query, ret_key, ret_value = tuple(
        ((running * row_scale[:, None]).astype(jnp.bfloat16) for running in projected)
    )
    head_count = stick_offset.shape[0]
    head_width = stick_query.shape[1] // head_count
    first_pos = lax.axis_index("sp") * tok_rows
    query_pos = first_pos + jnp.arange(tok_rows, dtype=jnp.int32)
    queries = stick_query.reshape(tok_rows, head_count, head_width)
    key_span = 4 * tok_rows
    keys_all, values_all = (
        lax.all_gather(stick_key, "sp", axis=0, tiled=True),
        lax.all_gather(stick_value, "sp", axis=0, tiled=True),
    )
    stick_total = sweep_keys(keys_all, values_all, queries, query_pos, stick_offset, key_span)
    stick_local = jnp.sum(jnp.square(stick_total), axis=(1, 2))
    stick_squares = lax.psum(stick_local, "tp")
    stick_scale = lax.rsqrt(stick_squares / (STICK_HEADS * STICK_DIM) + epsilon)
    stick_normed = (
        stick_total.reshape(tok_rows, head_count * head_width) * stick_scale[:, None] * stick_gain
    ).astype(jnp.bfloat16)
    state_full = lax.all_gather(initial_state, "sp", axis=1, tiled=True)
    ret_heads = ret_log_decay.shape[0]
    ret_width = ret_query.shape[1] // ret_heads
    turned_query = rotate(
        ret_query.reshape(tok_rows, ret_heads, ret_width).astype(jnp.float32), query_pos
    )
    turned_key = rotate(
        ret_key.reshape(tok_rows, ret_heads, ret_width).astype(jnp.float32), query_pos
    ) * ret_width ** (-0.5)
    ret_values = ret_value.reshape(tok_rows, ret_heads, ret_width).astype(jnp.float32)
    local_pos = jnp.arange(tok_rows, dtype=jnp.float32)
    distance = local_pos[:, None] - local_pos[None, :]
    decay_mask = jnp.where(
        distance[None] >= 0.0,
        jnp.exp(ret_log_decay[:, None, None] * jnp.maximum(distance, 0.0)[None]),
        0.0,
    )
    highest = lax.Precision.HIGHEST
    scores = jnp.einsum("thd,shd->hts", turned_query, turned_key, precision=highest) * decay_mask
    inner_part = jnp.einsum("hts,she->the", scores, ret_values, precision=highest)
    key_decay = jnp.exp(ret_log_decay[None, :] * (tok_rows - 1.0 - local_pos[:, None]))
    own_state = jnp.einsum(
        "shd,she->hde", turned_key * key_decay[:, :, None], ret_values, precision=highest
    )
    block_decay = jnp.exp(ret_log_decay * tok_rows)

    def join_states(earlier, later):
        return (earlier[0] * later[1][:, None, None] + later[0], earlier[1] * later[1])

    prefix_state, _ = entering_2(
        (own_state, block_decay),
        "sp",
        join_states,
        (jnp.zeros_like(own_state), jnp.ones_like(block_decay)),
    )
    entering = (
        prefix_state
        + jnp.exp(ret_log_decay * first_pos.astype(jnp.float32))[:, None, None] * state_full
    )
    query_decay = jnp.exp(ret_log_decay[None, :] * (local_pos[:, None] + 1.0))
    cross_part = (
        jnp.einsum("thd,hde->the", turned_query, entering, precision=highest)
        * query_decay[:, :, None]
    )
    ret_total = inner_part + cross_part
    centered = ret_total - jnp.mean(ret_total, axis=2, keepdims=True)
    normed = centered * lax.rsqrt(jnp.mean(centered * centered, axis=2, keepdims=True) + epsilon)
    ret_normed = (normed.reshape(tok_rows, ret_heads * ret_width) * ret_gain).astype(jnp.bfloat16)
    stick_cols, ret_cols = (
        lax.all_gather(stick_out_w, "sp", axis=1, tiled=True),
        lax.all_gather(ret_out_w, "sp", axis=1, tiled=True),
    )
    stick_part = jnp.dot(stick_normed, stick_cols, preferred_element_type=jnp.float32)
    return lax.psum_scatter(
        (stick_part + jnp.dot(ret_normed, ret_cols, preferred_element_type=jnp.float32)).astype(
            jnp.bfloat16
        ),
        "tp",
        scatter_dimension=0,
        tiled=True,
    )


def solution(mesh):
    in_specs = (
        P("sp", "tp"),
        P("tp"),
        P(None, "tp"),
        P(None, "tp"),
        P(None, "tp"),
        P(None, "tp"),
        P(None, "tp"),
        P(None, "tp"),
        P("tp"),
        P("tp"),
        P("tp", "sp", None),
        P("tp"),
        P("tp"),
        P("tp", "sp"),
        P("tp", "sp"),
    )
    out_specs = P(("sp", "tp"), None)
    return jax.shard_map(body, mesh=mesh, in_specs=in_specs, out_specs=out_specs, check_vma=False)
```

profile of v0, /device:TPU:0, one launch (start us, length us, event | category | flops | bytes accessed | tf_op | source)
XLA Modules:
  0.0 597.4 jit_solution(9106212903124527146)
XLA Ops:
  13.1 7.5 %all-gather.11.cloned.1.call-done = bf16[256,2048]{1,0:T(8,128)(2,1)} async-done(((bf16[256,1024]{1,0:T(8,128)(2,1)}), bf16[256,2048]{1,0:T(8,128)(2,1)}) %all-gather.11.cloned.1.call-update) | async-done | bytes 1048592 | tf_op jit(solution)/shard_map/all_gather | solution.py:117
  23.5 3.0 fusion.30
  27.3 3.4 fusion.26
  31.2 4.0 fusion.28
  46.4 43.1 %all-reduce = f32[64]{0:T(128)S(1)} all-reduce(f32[64]{0:T(128)S(1)} %get-tuple-element.346), channel_id=3, replica_groups=mesh['sp'=16,'tp'=2] {'sp'}, use_global_device_ids=true, to_apply=%add | all-reduce | flops 64 | bytes 512
  94.2 6.5 %all-gather.13.cloned.1.call-done = bf16[4096,512]{1,0:T(8,128)(2,1)} async-done(((bf16[256,512]{1,0:T(8,128)(2,1)}), bf16[4096,512]{1,0:T(8,128)(2,1)}) %all-gather.13.cloned.1.call-update) | async-done | bytes 4194320 | tf_op jit(solution)/shard_map/all_gather | solution.py:135
  100.7 77.1 %all-gather.15.cloned.1.call-done = bf16[4096,512]{1,0:T(8,128)(2,1)} async-done(((bf16[256,512]{1,0:T(8,128)(2,1)}), bf16[4096,512]{1,0:T(8,128)(2,1)}) %all-gather.15.cloned.1.call-update) | async-done | bytes 4194320 | tf_op jit(solution)/shard_map/all_gather | solution.py:134
  178.7 34.5 %while.29 = (s32[]{:T(128)}, f32[256,4,128]{0,2,1:T(8,128)}, f32[4,256]{1,0:T(4,128)S(1)}, s32[]{:T(128)}, s32[]{:T(128)}, /*index=5*/bf16[4096,512]{1,0:T(8,128...) while((s32[]{:T(128)}, f32[256,4,128]{0,2,1:T(8,128)}, ...), condition=%wide.region_6.7_spmd.clone, body=%wide.region_2.6_spmd.clone.sunk | while | flops 707463424 | bytes 96735608 | solution.py:91
  181.8 6.3 %fusion.89 = (f32[4,256]{1,0:T(4,128)S(1)}, f32[4,256,1024]{1,2,0:T(8,128)S(1)}, f32[4,1024,256]{2,1,0:T(8,128)}) fusion(f32[4]{0:T(128)S(1)} %get-tuple-element.519, pred[256,1024]{0,1:T(8,128)(4,1)S(1)} %compare_and_fusion.2, bf16[1024,4,128]{0,2,1:T(8,128)(2,1)S(1)} %bitcast.121, bf16[256,4,128]{2,0,1:T(8,128)(2,1)} %get-tuple-element.518), kind=kOutput, calls=%fused_computation.33.clone.1 | convolution fusion | flops 279968768 | bytes 9965584 | tf_op jit(solution)/shard_map/while/body/thd,shd->hts/dot_general | solution.py:48
  188.1 10.1 %fusion.90 = f32[4,256,8,128]{1,2,3,0:T(8,128)S(1)} fusion(f32[4,256,8,128]{1,3,2,0:T(8,128)S(1)} %bitcast.119), kind=kOutput, calls=%fused_computation.20.clone.1 | output fusion | flops 133169152 | bytes 8388608 | tf_op jit(solution)/shard_map/reduce-window.4
  205.2 6.6 %fusion.91 = bf16[4,256,1024]{1,2,0:T(8,128)(2,1)S(1)} fusion(f32[4,256,8,128]{1,3,2,0:T(8,128)S(1)} %copy.98, f32[4,1024,256]{2,1,0:T(8,128)S(1)} %copy-done.3, f32[4,256]{1,0:T(4,128)S(1)} %get-tuple-element.498, f32[4]{0:T(128)S(1)} %get-tuple-element.519, pred[256,1024]{0,1:T(8,128)(4,1)S(1)} %compare_and_fusion.2), kind=kLoop, calls=%fused_computation.8.clone.1 | loop fusion | flops 24117248 | bytes 10752016 | tf_op jit(solution)/shard_map/while/body/convert_element_type | solution.py:55
  218.2 151.9 %all-gather.23.cloned.1.call-done = f32[64,256,256]{2,1,0:T(8,128)} async-done(((f32[4,256,256]{2,1,0:T(8,128)}), f32[64,256,256]{2,1,0:T(8,128)}) %all-gather.23.cloned.1.call-update) | async-done | bytes 16777232 | tf_op jit(solution)/shard_map/all_gather | solution.py:15
  370.1 41.3 %while.30 = (s32[]{:T(128)}, f32[4,256,256]{2,1,0:T(8,128)}, s32[]{:T(128)}, f32[16,4]{1,0:T(8,128)S(1)}, f32[16,4,256,256]{3,2,1,0:T(8,128)}, /*index=5*/s32[]{:T(128)}, s32[]{:T(128)}) while((s32[]{:T(128)}, f32[4,256,256]{2,1,0:T(8,128)}, s32[]{:T(128)}, f32[16,4]{1,0:T(8,128)S(1)}, f32[16,4,256,256]{3,2,1,0:T(8,128)}, ...), condition=%wide.region_10.11_spmd.clone, body=%wide.region_9.10_spmd.clone.sunk | while | flops 1048580 | bytes 3145889 | solution.py:24
  378.2 2.8 fusion.93
  383.7 2.8 fusion.93
  394.7 2.8 fusion.93
  403.1 2.8 fusion.93
  411.3 14.5 %all-gather.19.cloned.1.call-done = f32[4,256,256]{2,1,0:T(8,128)} async-done(((f32[4,16,256]{2,1,0:T(8,128)}), f32[4,256,256]{2,1,0:T(8,128)}) %all-gather.19.cloned.1.call-update) | async-done | bytes 1048592 | tf_op jit(solution)/shard_map/all_gather | solution.py:144
  425.8 3.5 fusion.57
  429.8 86.2 %all-gather.21.cloned.1.call-done = bf16[1024,2048]{1,0:T(8,128)(2,1)} async-done(((bf16[1024,128]{1,0:T(8,128)(2,1)}), bf16[1024,2048]{1,0:T(8,128)(2,1)}) %all-gather.21.cloned.1.call-update) | async-done | bytes 4194320 | tf_op jit(solution)/shard_map/all_gather | solution.py:194
  516.0 4.9 fusion.58
  520.9 58.9 %all-gather.17.cloned.1.call-done = bf16[512,2048]{1,0:T(8,128)(2,1)} async-done(((bf16[512,128]{1,0:T(8,128)(2,1)}), bf16[512,2048]{1,0:T(8,128)(2,1)}) %all-gather.17.cloned.1.call-update) | async-done | bytes 2097168 | tf_op jit(solution)/shard_map/all_gather | solution.py:193
  579.8 3.9 fusion.21
  583.8 6.7 %reduce-scatter.2.cloned.1.call-done = bf16[128,2048]{1,0:T(8,128)(2,1)} async-done(((bf16[256,2048]{1,0:T(8,128)(2,1)}), bf16[128,2048]{1,0:T(8,128)(2,1)}) %reduce-scatter.2.cloned.1.call-update) | async-done | bytes 524304 | tf_op jit(solution)/shard_map/reduce_scatter | solution.py:197
  (138 shorter events, 72.9 us)
Async XLA Ops:
  6.5 14.1 %copy-start = (bf16[2048,512]{1,0:T(8,128)(2,1)S(1)}, bf16[2048,512]{1,0:T(8,128)(2,1)}, u32[]{:S(2)}) copy-start(bf16[2048,512]{1,0:T(8,128)(2,1)} %param.23) | copy-start | bytes 6291460
  6.5 14.1 %all-gather.11.cloned.1.call-start = ((), (), s32[]{:S(2)}) async-start(), calls=%async_computation.1 | async-start | bytes 1572864 | tf_op jit(solution)/shard_map/all_gather | solution.py:117
  7.3 93.4 %all-gather.13.cloned.1.call-start = ((), (), s32[]{:S(2)}) async-start(), calls=%async_computation.2 | async-start | bytes 4456448 | tf_op jit(solution)/shard_map/all_gather | solution.py:135
  13.1 13.5 %copy-start.14 = (f32[4]{0:T(128)S(1)}, f32[4]{0:T(128)}, u32[]{:S(2)}) copy-start(f32[4]{0:T(128)} %param.28) | copy-start | bytes 52
  20.7 2.8 copy-start.17
  23.4 154.4 %all-gather.15.cloned.1.call-start = ((), (), s32[]{:S(2)}) async-start(), calls=%async_computation.3 | async-start | bytes 4456448 | tf_op jit(solution)/shard_map/all_gather | solution.py:134
  26.5 343.5 %all-gather.23.cloned.1.call-start = ((), (), s32[]{:S(2)}) async-start(), calls=%async_computation.8 | async-start | bytes 17825792 | tf_op jit(solution)/shard_map/all_gather | solution.py:15
  38.2 51.4 %copy-start.7 = (f32[256,4,128]{2,0,1:T(8,128)}, f32[256,4,128]{2,0,1:T(8,128)S(1)}, u32[]{:S(2)}) copy-start(f32[256,4,128]{2,0,1:T(8,128)S(1)} %get-tuple-element.333) | copy-start | bytes 1572868
  38.2 51.4 %copy-start.9 = (f32[256,4,128]{2,0,1:T(8,128)}, f32[256,4,128]{2,0,1:T(8,128)S(1)}, u32[]{:S(2)}) copy-start(f32[256,4,128]{2,0,1:T(8,128)S(1)} %get-tuple-element.334) | copy-start | bytes 1572868
  38.2 6.9 %copy-start.20 = (u32[32]{0:T(128)S(1)}, u32[32]{0:T(128)}, u32[]{:S(2)}) copy-start(u32[32]{0:T(128)} %constant.118) | copy-start | bytes 388
  41.7 384.1 %all-gather.19.cloned.1.call-start = ((), (), s32[]{:S(2)}) async-start(), calls=%async_computation.5 | async-start | bytes 1114112 | tf_op jit(solution)/shard_map/all_gather | solution.py:144
  42.2 473.7 %all-gather.21.cloned.1.call-start = ((), (), s32[]{:S(2)}) async-start(), calls=%async_computation.6 | async-start | bytes 4456448 | tf_op jit(solution)/shard_map/all_gather | solution.py:194
  42.8 537.0 %all-gather.17.cloned.1.call-start = ((), (), s32[]{:S(2)}) async-start(), calls=%async_computation.4 | async-start | bytes 2228224 | tf_op jit(solution)/shard_map/all_gather | solution.py:193
  43.6 547.0 %reduce-scatter.2.cloned.1.call-start = ((), (), s32[]{:S(2)}) async-start(), calls=%async_computation.7 | async-start | bytes 1572864 | tf_op jit(solution)/shard_map/reduce_scatter | solution.py:197
  89.5 3.2 copy-start.16
  89.5 3.2 copy-start.19
  90.9 87.8 %copy-start.11 = (f32[4]{0:T(128)S(1)}, f32[4]{0:T(128)}, u32[]{:S(2)}) copy-start(f32[4]{0:T(128)} %param.27) | copy-start | bytes 52
  178.7 38.3 %copy-start.13 = (f32[512]{0:T(512)S(1)}, f32[512]{0:T(512)}, u32[]{:S(2)}) copy-start(f32[512]{0:T(512)} %param.30) | copy-start | bytes 6148
  205.2 6.6 %copy-start.4 = (f32[256,4,128]{0,2,1:T(8,128)S(1)}, f32[256,4,128]{0,2,1:T(8,128)}, u32[]{:S(2)}) copy-start(f32[256,4,128]{0,2,1:T(8,128)} %get-tuple-element.497) | copy-start | bytes 1572868 | tf_op jit(solution)/shard_map/while
  370.1 55.7 %copy-start.6 = (f32[256,4,256]{0,2,1:T(8,128)S(1)}, f32[256,4,256]{0,2,1:T(8,128)}, u32[]{:S(2)}) copy-start(f32[256,4,256]{0,2,1:T(8,128)} %convolution_bitcast_fusion.2) | copy-start | bytes 3145732
  370.1 55.7 %copy-start.8 = (f32[256,4,128]{2,0,1:T(8,128)S(1)}, f32[256,4,128]{2,0,1:T(8,128)}, u32[]{:S(2)}) copy-start(f32[256,4,128]{2,0,1:T(8,128)} %copy-done.7) | copy-start | bytes 1572868
  370.1 55.7 %copy-start.10 = (f32[256,4,128]{2,0,1:T(8,128)S(1)}, f32[256,4,128]{2,0,1:T(8,128)}, u32[]{:S(2)}) copy-start(f32[256,4,128]{2,0,1:T(8,128)} %copy-done.9) | copy-start | bytes 1572868
  425.8 3.8 copy-start.12
  516.0 74.6 %copy-start.1 = (bf16[2048,512]{1,0:T(8,128)(2,1)S(1)}, bf16[2048,512]{1,0:T(8,128)(2,1)}, u32[]{:S(2)}) copy-start(bf16[2048,512]{1,0:T(8,128)(2,1)} %param.23) | copy-start | bytes 6291460
  (5 other events, 9.7 us)
Sparse Core Ops, SparseCore 0:
  8.9 11.7 all-gather.10
  23.5 77.1 all-gather.12
  103.5 74.2 all-gather.14
  180.4 189.5 all-gather.22
  372.7 53.0 all-gather.18
  428.3 87.5 all-gather.20
  518.7 61.1 all-gather.16
  583.9 6.5 reduce-scatter.1
where the time goes:
time: 599 us; the launch traced here: 597 us
  waiting for transfers between devices  412 us (69%)
  other arithmetic  66 us (11%)
  blocking collectives  50.3 us (8%)
  matrix products  39.7 us (7%)
  between operations  15 us (3%)
  local copies, waits for them, and re-layouts  14 us (2%)
    all_gather x1, waiting for transfers between devices, entering_2(): pieces = jax.tree.map(lambda part: lax.all_gather(part, axis), value)  152 us
    all_gather x1, waiting for transfers between devices, body(): lax.all_gather(ret_out_w, 'sp', axis=1, tiled=True)  86.2 us
    all_gather x1, waiting for transfers between devices, body(): lax.all_gather(stick_key, 'sp', axis=0, tiled=True)  77.1 us
    all_gather x1, waiting for transfers between devices, body(): lax.all_gather(stick_out_w, 'sp', axis=1, tiled=True)  58.9 us
    unnamed x1, blocking collectives  43.1 us
    select_n x15, other arithmetic, hop(): jnp.where(position < mine, new, old)  41.1 us
    dot_general x6, matrix products, body(): jnp.dot(scaled, matrix, preferred_element_type=jnp.float32)  15.1 us
    all_gather x1, waiting for transfers between devices, body(): state_full = lax.all_gather(initial_state, 'sp', axis=1, tiled=True)  14.5 us
  transfers between devices with their start and end apart: 8, of which 8 were waited for; matrix products, arithmetic and copies ran while one was open for 18% of the time, Pallas kernels for 0%

commit v1 on v0

--- a/solution.py
+++ b/solution.py
@@ -8,6 +8,10 @@
 STICK_DIM = 128
 epsilon = 1e-06
 rope_base = 10000.0
+
+
+def advance_the_circles(array_here, mesh_dim, k_dim):
+    return jnp.concatenate(jax.lax.all_gather(array_here, mesh_dim), axis=k_dim)
 
 
 def entering_2(value, axis, join, neutral):
@@ -191,7 +195,7 @@
     ret_normed = (normed.reshape(tok_rows, ret_heads * ret_width) * ret_gain).astype(jnp.bfloat16)
     stick_cols, ret_cols = (
         lax.all_gather(stick_out_w, "sp", axis=1, tiled=True),
-        lax.all_gather(ret_out_w, "sp", axis=1, tiled=True),
+        advance_the_circles(ret_out_w, "sp", 1),
     )
     stick_part = jnp.dot(stick_normed, stick_cols, preferred_element_type=jnp.float32)
     return lax.psum_scatter(

time: 599 us -> 586 us (0.978)
  waiting for transfers between devices: 412 us -> 395 us
  local copies, waits for them, and re-layouts: 14 us -> 20.4 us
    all_gather x1, waiting for transfers between devices: 86.2 us -> 7.08 us  [advance_the_circles(): return jnp.concatenate(jax.lax.all_gather(array_here, mesh_dim), axis=k_dim)]
    all_gather x1, waiting for transfers between devices: 6.52 us -> 70.7 us  [body(): lax.all_gather(stick_value, 'sp', axis=0, tiled=True)]
    reshape x0 -> x1, local copies, waits for them, and re-layouts: none -> 6.39 us  [advance_the_circles(): return jnp.concatenate(jax.lax.all_gather(array_here, mesh_dim), axis=k_dim)]
  transfers between devices with their start and end apart: 8 -> 8, of which waited for: 8 -> 8; matrix products, arithmetic and copies ran while one was open for 18% -> 20% of each run, Pallas kernels for 0% -> 0%
where the time goes in v1:
time: 586 us; the launch traced here: 585 us
  waiting for transfers between devices  395 us (67%)
  other arithmetic  65.9 us (11%)
  blocking collectives  50.3 us (9%)
  matrix products  37.5 us (6%)
  local copies, waits for them, and re-layouts  20.4 us (3%)
  between operations  15 us (3%)
    all_gather x1, waiting for transfers between devices, entering_2(): pieces = jax.tree.map(lambda part: lax.all_gather(part, axis), value)  152 us
    all_gather x1, waiting for transfers between devices, body(): lax.all_gather(stick_key, 'sp', axis=0, tiled=True)  76.8 us
    all_gather x1, waiting for transfers between devices, body(): lax.all_gather(stick_value, 'sp', axis=0, tiled=True)  70.7 us
    all_gather x1, waiting for transfers between devices, body(): lax.all_gather(stick_out_w, 'sp', axis=1, tiled=True)  57.8 us
    unnamed x1, blocking collectives  43 us
    select_n x15, other arithmetic, hop(): jnp.where(position < mine, new, old)  41.1 us
    dot_general x6, matrix products, body(): jnp.dot(scaled, matrix, preferred_element_type=jnp.float32)  15.1 us
    all_gather x1, waiting for transfers between devices, body(): state_full = lax.all_gather(initial_state, 'sp', axis=1, tiled=True)  14.5 us
  transfers between devices with their start and end apart: 8, of which 8 were waited for; matrix products, arithmetic and copies ran while one was open for 20% of the time, Pallas kernels for 0%

profile of v1, /device:TPU:0, one launch (start us, length us, event | category | flops | bytes accessed | tf_op | source)
XLA Modules:
  0.0 584.7 jit_solution(15316957618424131384)
XLA Ops:
  13.9 6.8 %all-gather.12.cloned.1.call-done = bf16[256,2048]{1,0:T(8,128)(2,1)} async-done(((bf16[256,1024]{1,0:T(8,128)(2,1)}), bf16[256,2048]{1,0:T(8,128)(2,1)}) %all-gather.12.cloned.1.call-update) | async-done | bytes 1048592 | tf_op jit(solution)/shard_map/all_gather | solution.py:121
  23.5 3.0 fusion.30
  27.3 3.4 fusion.26
  31.2 3.9 fusion.28
  45.7 43.0 %all-reduce = f32[64]{0:T(128)S(1)} all-reduce(f32[64]{0:T(128)S(1)} %get-tuple-element.356), channel_id=3, replica_groups=mesh['sp'=16,'tp'=2] {'sp'}, use_global_device_ids=true, to_apply=%add | all-reduce | flops 64 | bytes 512
  93.5 7.1 %all-gather.24.cloned.1.call-done = bf16[16384,128]{1,0:T(8,128)(2,1)} async-done(((bf16[1024,128]{1,0:T(8,128)(2,1)}), bf16[16384,128]{1,0:T(8,128)(2,1)}) %all-gather.24.cloned.1.call-update) | async-done | bytes 4194320 | tf_op jit(solution)/shard_map/all_gather | solution.py:14
  100.6 6.4 %copy.75 = bf16[1024,16,128]{0,2,1:T(8,128)(2,1)} copy(bf16[1024,16,128]{2,0,1:T(8,128)(2,1)} %bitcast.123) | data formatting | bytes 8388608 | tf_op jit(solution)/shard_map/reshape | solution.py:14
  107.0 70.7 %all-gather.14.cloned.1.call-done = bf16[4096,512]{1,0:T(8,128)(2,1)} async-done(((bf16[256,512]{1,0:T(8,128)(2,1)}), bf16[4096,512]{1,0:T(8,128)(2,1)}) %all-gather.14.cloned.1.call-update) | async-done | bytes 4194320 | tf_op jit(solution)/shard_map/all_gather | solution.py:139
  177.7 76.8 %all-gather.16.cloned.1.call-done = bf16[4096,512]{1,0:T(8,128)(2,1)} async-done(((bf16[256,512]{1,0:T(8,128)(2,1)}), bf16[4096,512]{1,0:T(8,128)(2,1)}) %all-gather.16.cloned.1.call-update) | async-done | bytes 4194320 | tf_op jit(solution)/shard_map/all_gather | solution.py:138
  255.5 34.5 %while.29 = (s32[]{:T(128)}, f32[256,4,128]{0,2,1:T(8,128)}, f32[4,256]{1,0:T(4,128)S(1)}, s32[]{:T(128)}, s32[]{:T(128)}, /*index=5*/bf16[4096,512]{1,0:T(8,128...) while((s32[]{:T(128)}, f32[256,4,128]{0,2,1:T(8,128)}, ...), condition=%wide.region_6.7_spmd.clone, body=%wide.region_2.6_spmd.clone.sunk | while | flops 707463424 | bytes 96735608 | solution.py:95
  258.6 6.3 %fusion.88 = (f32[4,256]{1,0:T(4,128)S(1)}, f32[4,256,1024]{1,2,0:T(8,128)S(1)}, f32[4,1024,256]{2,1,0:T(8,128)}) fusion(f32[4]{0:T(128)S(1)} %get-tuple-element.529, pred[256,1024]{0,1:T(8,128)(4,1)S(1)} %compare_and_fusion.2, bf16[1024,4,128]{0,2,1:T(8,128)(2,1)S(1)} %bitcast.122, bf16[256,4,128]{2,0,1:T(8,128)(2,1)} %get-tuple-element.528), kind=kOutput, calls=%fused_computation.33.clone.1 | convolution fusion | flops 279968768 | bytes 9965584 | tf_op jit(solution)/shard_map/while/body/thd,shd->hts/dot_general | solution.py:52
  264.9 10.1 %fusion.89 = f32[4,256,8,128]{1,2,3,0:T(8,128)S(1)} fusion(f32[4,256,8,128]{1,3,2,0:T(8,128)S(1)} %bitcast.120), kind=kOutput, calls=%fused_computation.20.clone.1 | output fusion | flops 133169152 | bytes 8388608 | tf_op jit(solution)/shard_map/reduce-window.4
  282.0 6.6 %fusion.90 = bf16[4,256,1024]{1,2,0:T(8,128)(2,1)S(1)} fusion(f32[4,256,8,128]{1,3,2,0:T(8,128)S(1)} %copy.115, f32[4,1024,256]{2,1,0:T(8,128)S(1)} %copy-done.3, f32[4,256]{1,0:T(4,128)S(1)} %get-tuple-element.508, f32[4]{0:T(128)S(1)} %get-tuple-element.529, pred[256,1024]{0,1:T(8,128)(4,1)S(1)} %compare_and_fusion.2), kind=kLoop, calls=%fused_computation.8.clone.1 | loop fusion | flops 24117248 | bytes 10752016 | tf_op jit(solution)/shard_map/while/body/convert_element_type | solution.py:59
  295.0 151.9 %all-gather.22.cloned.1.call-done = f32[64,256,256]{2,1,0:T(8,128)} async-done(((f32[4,256,256]{2,1,0:T(8,128)}), f32[64,256,256]{2,1,0:T(8,128)}) %all-gather.22.cloned.1.call-update) | async-done | bytes 16777232 | tf_op jit(solution)/shard_map/all_gather | solution.py:19
  446.9 41.2 %while.30 = (s32[]{:T(128)}, f32[4,256,256]{2,1,0:T(8,128)}, s32[]{:T(128)}, f32[16,4]{1,0:T(8,128)S(1)}, f32[16,4,256,256]{3,2,1,0:T(8,128)}, /*index=5*/s32[]{:T(128)}, s32[]{:T(128)}) while((s32[]{:T(128)}, f32[4,256,256]{2,1,0:T(8,128)}, s32[]{:T(128)}, f32[16,4]{1,0:T(8,128)S(1)}, f32[16,4,256,256]{3,2,1,0:T(8,128)}, ...), condition=%wide.region_10.11_spmd.clone, body=%wide.region_9.10_spmd.clone.sunk | while | flops 1048580 | bytes 3145889 | solution.py:28
  455.0 2.8 fusion.92
  460.5 2.7 fusion.92
  471.5 2.8 fusion.92
  479.8 2.8 fusion.92
  488.1 14.5 %all-gather.20.cloned.1.call-done = f32[4,256,256]{2,1,0:T(8,128)} async-done(((f32[4,16,256]{2,1,0:T(8,128)}), f32[4,256,256]{2,1,0:T(8,128)}) %all-gather.20.cloned.1.call-update) | async-done | bytes 1048592 | tf_op jit(solution)/shard_map/all_gather | solution.py:148
  502.6 3.7 fusion.56
  509.3 57.8 %all-gather.18.cloned.1.call-done = bf16[512,2048]{1,0:T(8,128)(2,1)} async-done(((bf16[512,128]{1,0:T(8,128)(2,1)}), bf16[512,2048]{1,0:T(8,128)(2,1)}) %all-gather.18.cloned.1.call-update) | async-done | bytes 2097168 | tf_op jit(solution)/shard_map/all_gather | solution.py:197
  567.1 3.9 fusion.21
  571.1 6.7 %reduce-scatter.2.cloned.1.call-done = bf16[128,2048]{1,0:T(8,128)(2,1)} async-done(((bf16[256,2048]{1,0:T(8,128)(2,1)}), bf16[128,2048]{1,0:T(8,128)(2,1)}) %reduce-scatter.2.cloned.1.call-update) | async-done | bytes 524304 | tf_op jit(solution)/shard_map/reduce_scatter | solution.py:201
  (141 shorter events, 75.6 us)
Async XLA Ops:
  6.5 14.1 %copy-start = (bf16[2048,512]{1,0:T(8,128)(2,1)S(1)}, bf16[2048,512]{1,0:T(8,128)(2,1)}, u32[]{:S(2)}) copy-start(bf16[2048,512]{1,0:T(8,128)(2,1)} %param.23) | copy-start | bytes 6291460
  6.5 14.1 %all-gather.12.cloned.1.call-start = ((), (), s32[]{:S(2)}) async-start(), calls=%async_computation.1 | async-start | bytes 1572864 | tf_op jit(solution)/shard_map/all_gather | solution.py:121
  7.3 93.4 %all-gather.24.cloned.1.call-start = ((), (), s32[]{:S(2)}) async-start(), calls=%async_computation.8 | async-start | bytes 4456448 | tf_op jit(solution)/shard_map/all_gather | solution.py:14
  8.0 169.7 %all-gather.14.cloned.1.call-start = ((), (), s32[]{:S(2)}) async-start(), calls=%async_computation.2 | async-start | bytes 4456448 | tf_op jit(solution)/shard_map/all_gather | solution.py:139
  13.9 12.7 %copy-start.15 = (f32[4]{0:T(128)S(1)}, f32[4]{0:T(128)}, u32[]{:S(2)}) copy-start(f32[4]{0:T(128)} %param.28) | copy-start | bytes 52
  23.4 231.2 %all-gather.16.cloned.1.call-start = ((), (), s32[]{:S(2)}) async-start(), calls=%async_computation.3 | async-start | bytes 4456448 | tf_op jit(solution)/shard_map/all_gather | solution.py:138
  26.5 420.4 %all-gather.22.cloned.1.call-start = ((), (), s32[]{:S(2)}) async-start(), calls=%async_computation.7 | async-start | bytes 17825792 | tf_op jit(solution)/shard_map/all_gather | solution.py:19
  38.2 50.7 %copy-start.8 = (f32[256,4,128]{2,0,1:T(8,128)}, f32[256,4,128]{2,0,1:T(8,128)S(1)}, u32[]{:S(2)}) copy-start(f32[256,4,128]{2,0,1:T(8,128)S(1)} %get-tuple-element.343) | copy-start | bytes 1572868
  38.2 50.8 %copy-start.10 = (f32[256,4,128]{2,0,1:T(8,128)}, f32[256,4,128]{2,0,1:T(8,128)S(1)}, u32[]{:S(2)}) copy-start(f32[256,4,128]{2,0,1:T(8,128)S(1)} %get-tuple-element.344) | copy-start | bytes 1572868
  38.2 6.2 %copy-start.21 = (u32[32]{0:T(128)S(1)}, u32[32]{0:T(128)}, u32[]{:S(2)}) copy-start(u32[32]{0:T(128)} %constant.118) | copy-start | bytes 388
  38.2 50.7 %copy-start.13 = (f32[1024]{0:T(1024)S(1)}, f32[1024]{0:T(1024)}, u32[]{:S(2)}) copy-start(f32[1024]{0:T(1024)} %param.31) | copy-start | bytes 12292
  41.7 460.9 %all-gather.20.cloned.1.call-start = ((), (), s32[]{:S(2)}) async-start(), calls=%async_computation.5 | async-start | bytes 1114112 | tf_op jit(solution)/shard_map/all_gather | solution.py:148
  42.2 524.9 %all-gather.18.cloned.1.call-start = ((), (), s32[]{:S(2)}) async-start(), calls=%async_computation.4 | async-start | bytes 2228224 | tf_op jit(solution)/shard_map/all_gather | solution.py:197
  43.0 534.8 %reduce-scatter.2.cloned.1.call-start = ((), (), s32[]{:S(2)}) async-start(), calls=%async_computation.6 | async-start | bytes 1572864 | tf_op jit(solution)/shard_map/reduce_scatter | solution.py:201
  88.9 3.2 copy-start.17
  88.9 3.2 copy-start.20
  100.6 154.8 %copy-start.12 = (f32[4]{0:T(128)S(1)}, f32[4]{0:T(128)}, u32[]{:S(2)}) copy-start(f32[4]{0:T(128)} %param.27) | copy-start | bytes 52
  255.5 38.3 %copy-start.14 = (f32[512]{0:T(512)S(1)}, f32[512]{0:T(512)}, u32[]{:S(2)}) copy-start(f32[512]{0:T(512)} %param.30) | copy-start | bytes 6148
  282.0 6.6 %copy-start.4 = (f32[256,4,128]{0,2,1:T(8,128)S(1)}, f32[256,4,128]{0,2,1:T(8,128)}, u32[]{:S(2)}) copy-start(f32[256,4,128]{0,2,1:T(8,128)} %get-tuple-element.507) | copy-start | bytes 1572868 | tf_op jit(solution)/shard_map/while
  446.9 55.7 %copy-start.7 = (f32[256,4,256]{0,2,1:T(8,128)S(1)}, f32[256,4,256]{0,2,1:T(8,128)}, u32[]{:S(2)}) copy-start(f32[256,4,256]{0,2,1:T(8,128)} %convolution_bitcast_fusion.2) | copy-start | bytes 3145732
  446.9 55.7 %copy-start.9 = (f32[256,4,128]{2,0,1:T(8,128)S(1)}, f32[256,4,128]{2,0,1:T(8,128)}, u32[]{:S(2)}) copy-start(f32[256,4,128]{2,0,1:T(8,128)} %copy-done.8) | copy-start | bytes 1572868
  446.9 55.7 %copy-start.11 = (f32[256,4,128]{2,0,1:T(8,128)S(1)}, f32[256,4,128]{2,0,1:T(8,128)}, u32[]{:S(2)}) copy-start(f32[256,4,128]{2,0,1:T(8,128)} %copy-done.10) | copy-start | bytes 1572868
  502.6 4.1 copy-start.6
  506.6 71.2 %copy-start.1 = (bf16[2048,512]{1,0:T(8,128)(2,1)S(1)}, bf16[2048,512]{1,0:T(8,128)(2,1)}, u32[]{:S(2)}) copy-start(bf16[2048,512]{1,0:T(8,128)(2,1)} %param.23) | copy-start | bytes 6291460
  (6 other events, 12.6 us)
Sparse Core Ops, SparseCore 0:
  8.9 11.7 all-gather.11
  23.4 77.1 all-gather.23
  103.4 74.3 all-gather.13
  180.4 74.1 all-gather.15
  257.2 189.6 all-gather.21
  449.5 53.0 all-gather.19
  505.3 61.8 all-gather.17
  571.2 6.5 reduce-scatter.1
